TPU v7x, 32 devices: a whole 2x2x4 slice. The times are simulated.
32 devices in a mesh: sp: 4 (over y, core), dp: 8 (over z, x).
Axes of the slice: x: 2, y: 2, z: 4, core: 2. Of those that a mesh axis runs over, the one named last changes fastest.
Arguments:
- standardized_block_source: bfloat16 [16, 256, 2064], P('dp', 'sp'), may hold values from -6 to 6
- forgetting_narrowing_matrix: bfloat16 [2064, 32], P('dp'), may hold values from -0.125 to 0.125
- forgetting_widening_matrix: bfloat16 [32, 1024], replicated, may hold values from -1 to 1
- forgetting_offset_vector: float32 [1024], replicated, may hold values from -1.5 to 6.5
- probe_vectors: bfloat16 [128, 256, 128], P(('dp', 'sp')), may hold values from -6 to 6
- address_vectors: bfloat16 [128, 256, 128], P(('dp', 'sp')), may hold values from -6 to 6
- payload_vectors: bfloat16 [128, 256, 256], P(('dp', 'sp')), may hold values from -6 to 6
- extra_channel_forgetting: float32 [128, 256], P(('dp', 'sp')), may hold values from -2.1 to 0
- blender_result_adjoint: bfloat16 [16, 256, 2048], P('dp', 'sp'), may hold values from -0.29882812 to 0.29882812
Outputs:
- grad_queries: bfloat16 [16, 256, 1024], P('dp', 'sp')
- grad_keys: bfloat16 [16, 256, 1024], P('dp', 'sp')
- grad_values: bfloat16 [16, 256, 2048], P('dp', 'sp')
- grad_input: bfloat16 [16, 256, 2064], P('dp', 'sp')
- grad_gate_down: float32 [2064, 32], P('dp')
- grad_gate_up: float32 [32, 1024], replicated
- grad_gate_bias: float32 [1024], replicated
All inputs are finite; a program needn't handle non-finite values.
Results may differ from a plain program's by a relative error of at most 0.0069.
Values may be sent and summed in bfloat16 or wider, within the bound.
A program may use at most 64 MiB of HBM per device.

v0:
```python
import jax
import jax.numpy as jnp
from jax import lax
from jax.sharding import PartitionSpec as P

HEADS = 8
ADDRESS_WIDTH = 128
PAYLOAD_WIDTH = 256
BLOCK = 64
retention_smoothing = 16.0


def head_forward(
    stream_probe_entries, stream_address_entries, stream_payload_entries, retention_coefficient
):
    length, key_width = stream_probe_entries.shape
    value_width = stream_payload_entries.shape[1]
    blocks = length // BLOCK
    middle = BLOCK // 2
    scaled = stream_probe_entries * key_width ** (-0.5)
    causal = jnp.tril(jnp.ones((BLOCK, BLOCK), dtype=bool))
    highest = lax.Precision.HIGHEST

    def advance(memory, pieces):
        query_block, key_block, value_block, decay_sums = pieces
        centre = decay_sums[middle]
        lifted_query = query_block * jnp.exp(decay_sums - centre[None, :])
        lowered_key = key_block * jnp.exp(centre[None, :] - decay_sums)
        raw_scores = jnp.dot(lifted_query, lowered_key.T, precision=highest)
        scores = jnp.where(causal, raw_scores, 0.0)
        within = jnp.dot(scores, value_block, precision=highest)
        carried = jnp.dot(query_block * jnp.exp(decay_sums), memory, precision=highest)
        ending = decay_sums[-1]
        fading = key_block * jnp.exp(ending[None, :] - decay_sums)
        memory = memory * jnp.exp(ending)[:, None] + jnp.dot(
            fading.T, value_block, precision=highest
        )
        return (memory, within + carried)

    def blocked(tensor):
        return tensor.reshape(blocks, BLOCK, tensor.shape[1])

    initial = jnp.zeros((key_width, value_width), jnp.float32)
    decay_sums = jnp.cumsum(blocked(retention_coefficient), axis=1)
    _, outputs = lax.scan(
        jax.checkpoint(advance),
        initial,
        (
            blocked(scaled),
            blocked(stream_address_entries),
            blocked(stream_payload_entries),
            decay_sums,
        ),
    )
    return outputs.reshape(length, value_width)


def stream_sensitivities(
    stream_probe_entries,
    stream_address_entries,
    stream_payload_entries,
    forgetting_logit_values,
    surplus_retention_loss,
    result_adjoint,
):

    def forward(query_in, key_in, value_in, retention_basis_components):
        retention_coefficient = (
            jax.nn.log_sigmoid(retention_basis_components) / retention_smoothing
            + surplus_retention_loss[:, None]
        )
        return head_forward(query_in, key_in, value_in, retention_coefficient)

    _, pullback = jax.vjp(
        forward,
        stream_probe_entries.astype(jnp.float32),
        stream_address_entries.astype(jnp.float32),
        stream_payload_entries.astype(jnp.float32),
        forgetting_logit_values,
    )
    query_grad, key_grad, value_grad, gate_grad = pullback(result_adjoint.astype(jnp.float32))
    return (
        query_grad.astype(jnp.bfloat16),
        key_grad.astype(jnp.bfloat16),
        value_grad.astype(jnp.bfloat16),
        gate_grad.astype(jnp.bfloat16),
    )


def on_device(
    standardized_block_source,
    forgetting_narrowing_matrix,
    forgetting_widening_matrix,
    forgetting_offset_vector,
    probe_vectors,
    address_vectors,
    payload_vectors,
    extra_channel_forgetting,
    blender_result_adjoint,
):
    seqs, local_len, model_width = standardized_block_source.shape
    tokens_dev = seqs * local_len
    contract = (((0,), (0,)), ((), ()))
    flat_input = standardized_block_source.reshape(tokens_dev, model_width)
    down_whole = lax.all_gather(forgetting_narrowing_matrix, "dp", axis=0, tiled=True)
    low_rank = jnp.dot(flat_input, down_whole, preferred_element_type=jnp.float32).astype(
        jnp.bfloat16
    )
    logit_by_position = (
        jnp.dot(low_rank, forgetting_widening_matrix, preferred_element_type=jnp.float32)
        + forgetting_offset_vector
    )
    pre_items = (
        logit_by_position.reshape(seqs, local_len, HEADS, ADDRESS_WIDTH)
        .transpose(0, 2, 1, 3)
        .reshape(seqs * HEADS, local_len, ADDRESS_WIDTH)
    )
    logit_by_stream = lax.all_to_all(pre_items, "sp", split_axis=0, concat_axis=1, tiled=True)
    cot_items = (
        blender_result_adjoint.reshape(seqs, local_len, HEADS, PAYLOAD_WIDTH)
        .transpose(0, 2, 1, 3)
        .reshape(seqs * HEADS, local_len, PAYLOAD_WIDTH)
    )
    adjoint_split_by_stream = lax.all_to_all(
        cot_items, "sp", split_axis=0, concat_axis=1, tiled=True
    )
    query_grad, key_grad, value_grad, gate_grad = jax.vmap(stream_sensitivities)(
        probe_vectors,
        address_vectors,
        payload_vectors,
        logit_by_stream,
        extra_channel_forgetting,
        adjoint_split_by_stream,
    )
    returned = (
        lax.all_to_all(query_grad, "sp", split_axis=1, concat_axis=0, tiled=True),
        lax.all_to_all(key_grad, "sp", split_axis=1, concat_axis=0, tiled=True),
        lax.all_to_all(value_grad, "sp", split_axis=1, concat_axis=0, tiled=True),
        lax.all_to_all(gate_grad, "sp", split_axis=1, concat_axis=0, tiled=True),
    )

    def to_tokens(tensor):
        columns = tensor.shape[2]
        return (
            tensor.reshape(seqs, HEADS, local_len, columns)
            .transpose(0, 2, 1, 3)
            .reshape(seqs, local_len, HEADS * columns)
        )

    gate_tokens = to_tokens(returned[3]).reshape(tokens_dev, HEADS * ADDRESS_WIDTH)
    low_grad = jnp.dot(
        gate_tokens, forgetting_widening_matrix.T, preferred_element_type=jnp.float32
    ).astype(jnp.bfloat16)
    incoming_sensitivity = jnp.dot(
        low_grad, down_whole.T, preferred_element_type=jnp.float32
    ).astype(jnp.bfloat16)
    up_term = lax.dot_general(low_rank, gate_tokens, contract, preferred_element_type=jnp.float32)
    bias_term = jnp.sum(gate_tokens.astype(jnp.float32), axis=0)
    partition_lines_count = forgetting_narrowing_matrix.shape[0]
    whole_term = lax.dot_general(flat_input, low_grad, contract, preferred_element_type=jnp.float32)
    combined_contraction, up_grad, bias_grad = lax.psum(
        (whole_term, up_term, bias_term), ("sp", "dp")
    )
    down_grad = lax.dynamic_slice_in_dim(
        combined_contraction, lax.axis_index("dp") * partition_lines_count, partition_lines_count, 0
    )
    return (
        to_tokens(returned[0]),
        to_tokens(returned[1]),
        to_tokens(returned[2]),
        incoming_sensitivity.reshape(seqs, local_len, model_width),
        down_grad,
        up_grad,
        bias_grad,
    )


def solution(mesh):
    placed = (
        P("dp", "sp", None),
        P("dp", None),
        P(),
        P(),
        P(("dp", "sp"), None, None),
        P(("dp", "sp"), None, None),
        P(("dp", "sp"), None, None),
        P(("dp", "sp"), None),
        P("dp", "sp", None),
    )
    return jax.shard_map(
        on_device,
        mesh=mesh,
        in_specs=placed,
        out_specs=(
            P("dp", "sp", None),
            P("dp", "sp", None),
            P("dp", "sp", None),
            P("dp", "sp", None),
            P("dp", None),
            P(),
            P(),
        ),
        check_vma=False,
    )
```

profile of v0, /device:TPU:8, one launch (start us, length us, event | category | flops | bytes accessed | tf_op | source)
XLA Modules:
  0.0 303.0 jit_solution(9182041822408000112)
XLA Ops:
  7.2 28.5 %all-gather = bf16[8,258,32]{1,2,0:T(8,128)(2,1)S(1)} all-gather(bf16[1,258,32]{1,2,0:T(8,128)(2,1)} %bitcast.296), channel_id=1, replica_groups=mesh['sp'=4,'dp'=8] {'dp'}, dimensions={0}, use_global_device_ids=true | all-gather | bytes 148608 | tf_op jit(solution)/shard_map/all_gather | solution.py:105
  36.2 1.1 fusion.27
  38.4 3.5 %all-to-all-start = ((f32[16,64,128]{2,1,0:T(8,128)}), f32[16,64,128]{2,1,0:T(8,128)S(1)}, u32[]{:S(2)}, u32[]{:S(2)}) async-start(f32[16,64,128]{2,1,0:T(8,128)} %bitcast.3), calls=%async_computation | async-start | bytes 1048576 | tf_op jit(solution)/shard_map/all_to_all | solution.py:118
  42.0 1.2 copy.147
  49.0 1.6 all-to-all-done
  51.4 4.2 %all-to-all-start.1 = ((bf16[16,64,256]{2,1,0:T(8,128)(2,1)}), bf16[16,64,256]{2,1,0:T(8,128)(2,1)}, u32[]{:S(2)}, u32[]{:S(2)}) async-start(bf16[16,64,256]{2,1,0:T(8,128)(2,1)} %bitcast.16), calls=%async_computation.1 | async-start | bytes 1048576 | tf_op jit(solution)/shard_map/all_to_all | solution.py:124
  57.0 1.2 reduce_window_sum.22
  59.3 10.3 %while.36 = (s32[]{:T(128)}, f32[4,128,256]{2,1,0:T(8,128)S(1)}, f32[4,4,128,256]{3,2,1,0:T(8,128)}, f32[4,4,64,128]{3,2,1,0:T(8,128)S(1)}, f32[4,4,64,128]{3,2,...) while((s32[]{:T(128)}, f32[4,128,256]{2,1,0:T(8,128)S(1)}, ...), condition=%wide.region_2.3_spmd.clone, body=%wide.region_1.2_spmd.clone.sunk | while | flops 101253120 | bytes 2897508 | solution.py:45
  60.2 1.6 convolution_add_fusion.6
  62.8 1.6 convolution_add_fusion.6
  65.4 1.6 convolution_add_fusion.6
  67.9 1.6 convolution_add_fusion.6
  70.4 2.1 convert.7
  75.1 38.5 %while.37 = (s32[]{:T(128)}, f32[4,128,256]{2,1,0:T(8,128)S(1)}, f32[4,4,64,128]{3,2,0,1:T(8,128)}, bf16[4,4,64,128]{3,2,0,1:T(8,128)(2,1)}, bf16[4,4,64,256]{3,...) while((s32[]{:T(128)}, f32[4,128,256]{2,1,0:T(8,128)S(1)}, ...), condition=%wide.region_8.9_spmd.clone, body=%wide.region_3.8_spmd.clone.sunk | while | flops 581210112 | bytes 23470384 | solution.py:45
  75.1 1.3 dynamic-slice_bitcast_fusion.17
  84.8 1.3 dynamic-slice_bitcast_fusion.17
  94.4 1.3 dynamic-slice_bitcast_fusion.17
  104.0 1.3 dynamic-slice_bitcast_fusion.17
  113.6 5.7 %reduce_window_sum.23 = f32[4,4,64,128]{3,2,1,0:T(8,128)S(1)} reduce-window(f32[4,4,64,128]{3,2,1,0:T(8,128)} %get-tuple-element.309, f32[]{:T(128)} %constant.99.clone.1), window={size=1x1x64x1 pad=0_0x0_0x0_63x0_0}, to_apply=%region_9.10 | reduce-window | flops 8257536 | bytes 1048580 | tf_op jit(solution)/shard_map/vmap(transpose(jvp(jit(cumsum))))/reduce_window_sum | solution.py:44
  120.8 3.6 %all-to-all-start.5 = ((bf16[4,256,128]{2,0,1:T(4,128)(2,1)}), bf16[4,256,128]{2,0,1:T(4,128)(2,1)S(1)}, u32[]{:S(2)}, u32[]{:S(2)}) async-start(bf16[4,256,128]{2,0,1:T(4,128)(2,1)} %copy.126), calls=%async_computation.5 | async-start | bytes 524288 | tf_op jit(solution)/shard_map/all_to_all | solution.py:139
  125.4 1.9 copy.116
  127.3 1.2 copy.121
  128.5 1.9 all-to-all-done.5
  130.3 3.4 %all-to-all-start.2 = ((bf16[4,256,128]{2,0,1:T(4,128)(2,1)}), bf16[4,256,128]{2,0,1:T(4,128)(2,1)S(1)}, u32[]{:S(2)}, u32[]{:S(2)}) async-start(bf16[4,256,128]{2,0,1:T(4,128)(2,1)} %copy.111), calls=%async_computation.2 | async-start | bytes 524288 | tf_op jit(solution)/shard_map/all_to_all | solution.py:136
  135.1 4.6 %all-to-all-done.2 = bf16[4,256,128]{2,0,1:T(4,128)(2,1)S(1)} async-done(((bf16[4,256,128]{2,0,1:T(4,128)(2,1)}), bf16[4,256,128]{2,0,1:T(4,128)(2,1)S(1)}, u32[]{:S(2)}, u32[]{:S(2)}) %all-to-all-start.2) | async-done | bytes 262176 | tf_op jit(solution)/shard_map/all_to_all | solution.py:136
  139.7 3.4 %all-to-all-start.3 = ((bf16[4,256,128]{2,0,1:T(4,128)(2,1)}), bf16[4,256,128]{2,0,1:T(4,128)(2,1)S(1)}, u32[]{:S(2)}, u32[]{:S(2)}) async-start(bf16[4,256,128]{2,0,1:T(4,128)(2,1)} %copy.116), calls=%async_computation.3 | async-start | bytes 524288 | tf_op jit(solution)/shard_map/all_to_all | solution.py:137
  143.5 5.6 %all-to-all-done.3 = bf16[4,256,128]{2,0,1:T(4,128)(2,1)S(1)} async-done(((bf16[4,256,128]{2,0,1:T(4,128)(2,1)}), bf16[4,256,128]{2,0,1:T(4,128)(2,1)S(1)}, u32[]{:S(2)}, u32[]{:S(2)}) %all-to-all-start.3) | async-done | bytes 262176 | tf_op jit(solution)/shard_map/all_to_all | solution.py:137
  149.1 3.5 %all-to-all-start.4 = ((bf16[4,256,256]{2,0,1:T(4,128)(2,1)}), bf16[4,256,256]{2,0,1:T(4,128)(2,1)S(1)}, u32[]{:S(2)}, u32[]{:S(2)}) async-start(bf16[4,256,256]{2,0,1:T(4,128)(2,1)} %copy.121), calls=%async_computation.4 | async-start | bytes 1048576 | tf_op jit(solution)/shard_map/all_to_all | solution.py:138
  154.7 43.5 %psum.23 = f32[1024]{0:T(1024)} all-reduce(f32[1024]{0:T(1024)S(1)} %bitcast.297), channel_id=1, replica_groups=mesh['sp'=4,'dp'=8] {'sp','dp'}, use_global_device_ids=true, to_apply=%region_13.14 | all-reduce | flops 1024 | bytes 8192 | tf_op jit(solution)/shard_map/psum | solution.py:161
  200.0 93.0 %all-reduce.5.cloned.1.call-done = (f32[2064,32]{0,1:T(8,128)}, f32[32,1024]{1,0:T(8,128)}) async-done(((f32[2064,32]{0,1:T(8,128)}, f32[32,1024]{1,0:T(8,128)}), (f32[2064,32]{0,1:T(8,128)}, f32[32,1024]{1,0:T(8,128)})) %all-reduce.5.cloned.1.call-update) | async-done | bytes 395280 | tf_op jit(solution)/shard_map/psum | solution.py:161
  293.0 1.5 constant_dynamic-slice_fusion
  294.6 1.6 copy.194
  (207 shorter events, 58.5 us)
Async XLA Ops:
  7.2 28.8 %copy-start = (bf16[2,64,2064]{2,1,0:T(8,128)(2,1)S(1)}, bf16[2,64,2064]{2,1,0:T(8,128)(2,1)}, u32[]{:S(2)}) copy-start(bf16[2,64,2064]{2,1,0:T(8,128)(2,1)} %param.13) | copy-start | bytes 1585156
  35.9 5.9 %copy-start.11 = (bf16[4,256,256]{2,1,0:T(8,128)(2,1)S(1)}, bf16[4,256,256]{2,1,0:T(8,128)(2,1)}, u32[]{:S(2)}) copy-start(bf16[4,256,256]{2,1,0:T(8,128)(2,1)} %param.19) | copy-start | bytes 1572868
  38.4 12.3 %all-to-all-start = ((f32[16,64,128]{2,1,0:T(8,128)}), f32[16,64,128]{2,1,0:T(8,128)S(1)}, u32[]{:S(2)}, u32[]{:S(2)}) async-start(f32[16,64,128]{2,1,0:T(8,128)} %bitcast.3), calls=%async_computation | async-start | bytes 1048576 | tf_op jit(solution)/shard_map/all_to_all | solution.py:118
  41.9 2.2 copy-start.12
  41.9 3.0 copy-start.15
  44.9 1.1 copy-start.10
  44.9 1.6 copy-start.6
  46.1 2.1 copy-start.13
  51.4 19.0 %all-to-all-start.1 = ((bf16[16,64,256]{2,1,0:T(8,128)(2,1)}), bf16[16,64,256]{2,1,0:T(8,128)(2,1)}, u32[]{:S(2)}, u32[]{:S(2)}) async-start(bf16[16,64,256]{2,1,0:T(8,128)(2,1)} %bitcast.16), calls=%async_computation.1 | async-start | bytes 1048576 | tf_op jit(solution)/shard_map/all_to_all | solution.py:124
  75.1 1.3 copy-start.1
  81.7 1.8 copy-start.7
  82.7 2.1 copy-start.2
  84.0 0.8 copy-start.8
  84.8 1.3 copy-start.1
  91.3 1.8 copy-start.7
  92.3 2.1 copy-start.2
  94.4 1.3 copy-start.1
  101.0 1.8 copy-start.7
  101.9 2.1 copy-start.2
  104.0 1.3 copy-start.1
  110.6 1.8 copy-start.7
  111.6 2.1 copy-start.2
  112.8 0.8 copy-start.8
  113.6 5.8 %copy-start.4 = (f32[4,4,64,128]{3,2,0,1:T(8,128)S(1)}, f32[4,4,64,128]{3,2,0,1:T(8,128)}, u32[]{:S(2)}) copy-start(f32[4,4,64,128]{3,2,0,1:T(8,128)} %copy.101) | copy-start | bytes 1572868
  119.3 5.1 %copy-start.3 = (f32[4,4,64,128]{3,2,0,1:T(8,128)S(1)}, f32[4,4,64,128]{3,2,0,1:T(8,128)}, u32[]{:S(2)}) copy-start(f32[4,4,64,128]{3,2,0,1:T(8,128)} %get-tuple-element.306) | copy-start | bytes 1572868
  119.4 7.8 %copy-start.9 = (bf16[4,4,64,256]{3,2,0,1:T(8,128)(2,1)S(1)}, bf16[4,4,64,256]{3,2,0,1:T(8,128)(2,1)}, u32[]{:S(2)}) copy-start(bf16[4,4,64,256]{3,2,0,1:T(8,128)(2,1)} %get-tuple-element.308) | copy-start | bytes 1572868
  120.8 9.5 %all-to-all-start.5 = ((bf16[4,256,128]{2,0,1:T(4,128)(2,1)}), bf16[4,256,128]{2,0,1:T(4,128)(2,1)S(1)}, u32[]{:S(2)}, u32[]{:S(2)}) async-start(bf16[4,256,128]{2,0,1:T(4,128)(2,1)} %copy.126), calls=%async_computation.5 | async-start | bytes 524288 | tf_op jit(solution)/shard_map/all_to_all | solution.py:139
  124.5 9.5 %copy-start.14 = (bf16[32,1024]{1,0:T(8,128)(2,1)S(1)}, bf16[32,1024]{1,0:T(8,128)(2,1)}, u32[]{:S(2)}) copy-start(bf16[32,1024]{1,0:T(8,128)(2,1)} %param.15) | copy-start | bytes 196612
  130.3 9.4 %all-to-all-start.2 = ((bf16[4,256,128]{2,0,1:T(4,128)(2,1)}), bf16[4,256,128]{2,0,1:T(4,128)(2,1)S(1)}, u32[]{:S(2)}, u32[]{:S(2)}) async-start(bf16[4,256,128]{2,0,1:T(4,128)(2,1)} %copy.111), calls=%async_computation.2 | async-start | bytes 524288 | tf_op jit(solution)/shard_map/all_to_all | solution.py:136
  139.7 9.4 %all-to-all-start.3 = ((bf16[4,256,128]{2,0,1:T(4,128)(2,1)}), bf16[4,256,128]{2,0,1:T(4,128)(2,1)S(1)}, u32[]{:S(2)}, u32[]{:S(2)}) async-start(bf16[4,256,128]{2,0,1:T(4,128)(2,1)} %copy.116), calls=%async_computation.3 | async-start | bytes 524288 | tf_op jit(solution)/shard_map/all_to_all | solution.py:137
  149.1 50.0 %all-to-all-start.4 = ((bf16[4,256,256]{2,0,1:T(4,128)(2,1)}), bf16[4,256,256]{2,0,1:T(4,128)(2,1)S(1)}, u32[]{:S(2)}, u32[]{:S(2)}) async-start(bf16[4,256,256]{2,0,1:T(4,128)(2,1)} %copy.121), calls=%async_computation.4 | async-start | bytes 1048576 | tf_op jit(solution)/shard_map/all_to_all | solution.py:138
  152.6 140.4 %all-reduce.5.cloned.1.call-start = ((), (), s32[]{:S(2)}) async-start(), calls=%async_computation.6 | async-start | bytes 819200 | tf_op jit(solution)/shard_map/psum | solution.py:161
  (3 other events, 2.4 us)
Sparse Core Ops, SparseCore 0:
  159.4 133.6 all-reduce.4
where the time goes:
time: 304 us; the launch traced here: 303 us
  waiting for transfers between devices  107 us (35%)
  blocking collectives  72 us (24%)
  local copies, waits for them, and re-layouts  36.1 us (12%)
  matrix products  30 us (10%)
  starting transfers between devices  21.5 us (7%)
  other arithmetic  21.5 us (7%)
  between operations  14.4 us (5%)
    psum x1, waiting for transfers between devices, on_device(): lax.psum((whole_term, up_term, bias_term), ('sp', 'dp'))  93 us
    psum x1, blocking collectives, on_device(): lax.psum((whole_term, up_term, bias_term), ('sp', 'dp'))  43.5 us
    all_gather x1, blocking collectives, on_device(): lax.all_gather(forgetting_narrowing_matrix, 'dp', axis=0, tiled=True)  28.5 us
    squeeze x20, local copies, waits for them, and re-layouts, head_forward(): lax.scan(jax.checkpoint(advance), initial, (blocked(scaled), blocked(stre...  13.2 us
    dot_general x12, matrix products, advance(): jnp.dot(fading.T, value_block, precision=highest)  11 us
    another operation x2, other arithmetic, head_forward(): decay_sums = jnp.cumsum(blocked(retention_coefficient), axis=1)  6.91 us
    dot_general x12, matrix products, advance(): raw_scores = jnp.dot(lifted_query, lowered_key.T, precision=highest)  6.88 us
    dynamic_update_slice x8, other arithmetic, head_forward(): lax.scan(jax.checkpoint(advance), initial, (blocked(scaled), blocked(stre...  6.55 us
  transfers between devices with their start and end apart: 7, of which 5 were waited for; matrix products, arithmetic and copies ran while one was open for 10% of the time, Pallas kernels for 0%

commit v1 on v0

--- a/solution.py
+++ b/solution.py
@@ -159,7 +159,7 @@
     partition_lines_count = forgetting_narrowing_matrix.shape[0]
     whole_term = lax.dot_general(flat_input, low_grad, contract, preferred_element_type=jnp.float32)
     combined_contraction, up_grad, bias_grad = lax.psum(
-        (whole_term, up_term, bias_term), ("sp", "dp")
+        lax.psum((whole_term, up_term, bias_term), "dp"), "sp"
     )
     down_grad = lax.dynamic_slice_in_dim(
         combined_contraction, lax.axis_index("dp") * partition_lines_count, partition_lines_count, 0

time: 304 us -> 272 us (0.89)
  waiting for transfers between devices: 107 us -> 88.3 us
  blocking collectives: 72 us -> 56.1 us
    psum x1 -> x2, waiting for transfers between devices: 93 us -> 75.1 us  [the longest x1 42.1 us: on_device(): lax.psum((whole_term, up_term, bias_term), 'dp')]
    psum x1 -> x2, blocking collectives: 43.5 us -> 27.6 us  [the longest x1 21.3 us: on_device(): lax.psum((whole_term, up_term, bias_term), 'dp')]
  transfers between devices with their start and end apart: 7 -> 8, of which waited for: 5 -> 6; matrix products, arithmetic and copies ran while one was open for 10% -> 11% of each run, Pallas kernels for 0% -> 0%
where the time goes in v1:
time: 272 us; the launch traced here: 269 us
  waiting for transfers between devices  88.3 us (32%)
  blocking collectives  56.1 us (21%)
  local copies, waits for them, and re-layouts  36.1 us (13%)
  matrix products  30 us (11%)
  starting transfers between devices  21.6 us (8%)
  other arithmetic  21.4 us (8%)
  between operations  14.4 us (5%)
    psum x1, waiting for transfers between devices, on_device(): lax.psum((whole_term, up_term, bias_term), 'dp')  42.1 us
    psum x1, waiting for transfers between devices, on_device(): lax.psum(lax.psum((whole_term, up_term, bias_term), 'dp'), 'sp')  33 us
    all_gather x1, blocking collectives, on_device(): lax.all_gather(forgetting_narrowing_matrix, 'dp', axis=0, tiled=True)  28.5 us
    psum x1, blocking collectives, on_device(): lax.psum((whole_term, up_term, bias_term), 'dp')  21.3 us
    squeeze x20, local copies, waits for them, and re-layouts, head_forward(): lax.scan(jax.checkpoint(advance), initial, (blocked(scaled), blocked(stre...  13.2 us
    dot_general x12, matrix products, advance(): jnp.dot(fading.T, value_block, precision=highest)  11 us
    another operation x2, other arithmetic, head_forward(): decay_sums = jnp.cumsum(blocked(retention_coefficient), axis=1)  6.91 us
    dot_general x12, matrix products, advance(): raw_scores = jnp.dot(lifted_query, lowered_key.T, precision=highest)  6.88 us
  transfers between devices with their start and end apart: 8, of which 6 were waited for; matrix products, arithmetic and copies ran while one was open for 11% of the time, Pallas kernels for 0%

profile of v1, /device:TPU:8, one launch (start us, length us, event | category | flops | bytes accessed | tf_op | source)
XLA Modules:
  0.0 268.7 jit_solution(10431426394592941532)
XLA Ops:
  7.2 28.5 %all-gather = bf16[8,258,32]{1,2,0:T(8,128)(2,1)S(1)} all-gather(bf16[1,258,32]{1,2,0:T(8,128)(2,1)} %bitcast.296), channel_id=1, replica_groups=mesh['sp'=4,'dp'=8] {'dp'}, dimensions={0}, use_global_device_ids=true | all-gather | bytes 148608 | tf_op jit(solution)/shard_map/all_gather | solution.py:105
  38.4 3.5 %all-to-all-start = ((f32[16,64,128]{2,1,0:T(8,128)}), f32[16,64,128]{2,1,0:T(8,128)S(1)}, u32[]{:S(2)}, u32[]{:S(2)}) async-start(f32[16,64,128]{2,1,0:T(8,128)} %bitcast.3), calls=%async_computation | async-start | bytes 1048576 | tf_op jit(solution)/shard_map/all_to_all | solution.py:118
  49.0 1.6 all-to-all-done
  51.4 4.1 %all-to-all-start.1 = ((bf16[16,64,256]{2,1,0:T(8,128)(2,1)}), bf16[16,64,256]{2,1,0:T(8,128)(2,1)}, u32[]{:S(2)}, u32[]{:S(2)}) async-start(bf16[16,64,256]{2,1,0:T(8,128)(2,1)} %bitcast.16), calls=%async_computation.1 | async-start | bytes 1048576 | tf_op jit(solution)/shard_map/all_to_all | solution.py:124
  57.0 1.2 reduce_window_sum.22
  59.3 10.3 %while.36 = (s32[]{:T(128)}, f32[4,128,256]{2,1,0:T(8,128)S(1)}, f32[4,4,128,256]{3,2,1,0:T(8,128)}, f32[4,4,64,128]{3,2,1,0:T(8,128)S(1)}, f32[4,4,64,128]{3,2,...) while((s32[]{:T(128)}, f32[4,128,256]{2,1,0:T(8,128)S(1)}, ...), condition=%wide.region_2.3_spmd.clone, body=%wide.region_1.2_spmd.clone.sunk | while | flops 101253120 | bytes 2897508 | solution.py:45
  60.2 1.6 convolution_add_fusion.6
  62.8 1.6 convolution_add_fusion.6
  65.4 1.6 convolution_add_fusion.6
  67.9 1.6 convolution_add_fusion.6
  70.4 2.1 convert.7
  75.1 38.5 %while.37 = (s32[]{:T(128)}, f32[4,128,256]{2,1,0:T(8,128)S(1)}, f32[4,4,64,128]{3,2,0,1:T(8,128)}, bf16[4,4,64,128]{3,2,0,1:T(8,128)(2,1)}, bf16[4,4,64,256]{3,...) while((s32[]{:T(128)}, f32[4,128,256]{2,1,0:T(8,128)S(1)}, ...), condition=%wide.region_8.9_spmd.clone, body=%wide.region_3.8_spmd.clone.sunk | while | flops 581210112 | bytes 23470384 | solution.py:45
  75.1 1.3 dynamic-slice_bitcast_fusion.17
  84.7 1.3 dynamic-slice_bitcast_fusion.17
  94.3 1.3 dynamic-slice_bitcast_fusion.17
  104.0 1.3 dynamic-slice_bitcast_fusion.17
  113.6 5.7 %reduce_window_sum.23 = f32[4,4,64,128]{3,2,1,0:T(8,128)S(1)} reduce-window(f32[4,4,64,128]{3,2,1,0:T(8,128)} %get-tuple-element.309, f32[]{:T(128)} %constant.99.clone.1), window={size=1x1x64x1 pad=0_0x0_0x0_63x0_0}, to_apply=%region_9.10 | reduce-window | flops 8257536 | bytes 1048580 | tf_op jit(solution)/shard_map/vmap(transpose(jvp(jit(cumsum))))/reduce_window_sum | solution.py:44
  120.8 3.6 %all-to-all-start.5 = ((bf16[4,256,128]{2,0,1:T(4,128)(2,1)}), bf16[4,256,128]{2,0,1:T(4,128)(2,1)S(1)}, u32[]{:S(2)}, u32[]{:S(2)}) async-start(bf16[4,256,128]{2,0,1:T(4,128)(2,1)} %copy.126), calls=%async_computation.5 | async-start | bytes 524288 | tf_op jit(solution)/shard_map/all_to_all | solution.py:139
  125.4 1.9 copy.116
  127.2 3.1 %all-to-all-done.5 = bf16[4,256,128]{2,0,1:T(4,128)(2,1)S(1)} async-done(((bf16[4,256,128]{2,0,1:T(4,128)(2,1)}), bf16[4,256,128]{2,0,1:T(4,128)(2,1)S(1)}, u32[]{:S(2)}, u32[]{:S(2)}) %all-to-all-start.5) | async-done | bytes 262176 | tf_op jit(solution)/shard_map/all_to_all | solution.py:139
  130.3 3.4 %all-to-all-start.2 = ((bf16[4,256,128]{2,0,1:T(4,128)(2,1)}), bf16[4,256,128]{2,0,1:T(4,128)(2,1)S(1)}, u32[]{:S(2)}, u32[]{:S(2)}) async-start(bf16[4,256,128]{2,0,1:T(4,128)(2,1)} %copy.111), calls=%async_computation.2 | async-start | bytes 524288 | tf_op jit(solution)/shard_map/all_to_all | solution.py:136
  135.1 4.6 %all-to-all-done.2 = bf16[4,256,128]{2,0,1:T(4,128)(2,1)S(1)} async-done(((bf16[4,256,128]{2,0,1:T(4,128)(2,1)}), bf16[4,256,128]{2,0,1:T(4,128)(2,1)S(1)}, u32[]{:S(2)}, u32[]{:S(2)}) %all-to-all-start.2) | async-done | bytes 262176 | tf_op jit(solution)/shard_map/all_to_all | solution.py:136
  139.7 3.4 %all-to-all-start.3 = ((bf16[4,256,128]{2,0,1:T(4,128)(2,1)}), bf16[4,256,128]{2,0,1:T(4,128)(2,1)S(1)}, u32[]{:S(2)}, u32[]{:S(2)}) async-start(bf16[4,256,128]{2,0,1:T(4,128)(2,1)} %copy.116), calls=%async_computation.3 | async-start | bytes 524288 | tf_op jit(solution)/shard_map/all_to_all | solution.py:137
  144.0 1.2 copy.121
  145.2 3.9 %all-to-all-done.3 = bf16[4,256,128]{2,0,1:T(4,128)(2,1)S(1)} async-done(((bf16[4,256,128]{2,0,1:T(4,128)(2,1)}), bf16[4,256,128]{2,0,1:T(4,128)(2,1)S(1)}, u32[]{:S(2)}, u32[]{:S(2)}) %all-to-all-start.3) | async-done | bytes 262176 | tf_op jit(solution)/shard_map/all_to_all | solution.py:137
  149.0 3.5 %all-to-all-start.4 = ((bf16[4,256,256]{2,0,1:T(4,128)(2,1)}), bf16[4,256,256]{2,0,1:T(4,128)(2,1)S(1)}, u32[]{:S(2)}, u32[]{:S(2)}) async-start(bf16[4,256,256]{2,0,1:T(4,128)(2,1)} %copy.121), calls=%async_computation.4 | async-start | bytes 1048576 | tf_op jit(solution)/shard_map/all_to_all | solution.py:138
  154.2 21.3 %psum.46 = f32[1024]{0:T(1024)S(1)} all-reduce(f32[1024]{0:T(1024)S(1)} %bitcast.297), channel_id=1, replica_groups=mesh['sp'=4,'dp'=8] {'dp'}, use_global_device_ids=true, to_apply=%region_15.16 | all-reduce | flops 1024 | bytes 8192 | tf_op jit(solution)/shard_map/psum | solution.py:162
  175.5 6.2 %psum.47 = f32[1024]{0:T(1024)} all-reduce(f32[1024]{0:T(1024)S(1)} %psum.46), channel_id=1, replica_groups=mesh['sp'=4,'dp'=8] {'sp'}, use_global_device_ids=true, to_apply=%region_16.17 | all-reduce | flops 1024 | bytes 8192 | tf_op jit(solution)/shard_map/psum | solution.py:161
  181.8 42.1 %all-reduce.7.cloned.1.call-done = (f32[2064,32]{0,1:T(8,128)}, f32[32,1024]{1,0:T(8,128)}) async-done(((f32[2064,32]{0,1:T(8,128)}, f32[32,1024]{1,0:T(8,128)}), (f32[2064,32]{0,1:T(8,128)}, f32[32,1024]{1,0:T(8,128)})) %all-reduce.7.cloned.1.call-update) | async-done | bytes 395280 | tf_op jit(solution)/shard_map/psum | solution.py:162
  225.7 33.0 %all-reduce.9.cloned.1.call-done = (f32[2064,32]{0,1:T(8,128)}, f32[32,1024]{1,0:T(8,128)}) async-done(((f32[2064,32]{0,1:T(8,128)}, f32[32,1024]{1,0:T(8,128)}), (f32[2064,32]{0,1:T(8,128)}, f32[32,1024]{1,0:T(8,128)})) %all-reduce.9.cloned.1.call-update) | async-done | bytes 395280 | tf_op jit(solution)/shard_map/psum | solution.py:161
  258.8 1.5 constant_dynamic-slice_fusion
  260.3 1.6 copy.196
  (211 shorter events, 60.8 us)
Async XLA Ops:
  7.2 28.8 %copy-start = (bf16[2,64,2064]{2,1,0:T(8,128)(2,1)S(1)}, bf16[2,64,2064]{2,1,0:T(8,128)(2,1)}, u32[]{:S(2)}) copy-start(bf16[2,64,2064]{2,1,0:T(8,128)(2,1)} %param.13) | copy-start | bytes 1585156
  35.9 5.9 %copy-start.11 = (bf16[4,256,256]{2,1,0:T(8,128)(2,1)S(1)}, bf16[4,256,256]{2,1,0:T(8,128)(2,1)}, u32[]{:S(2)}) copy-start(bf16[4,256,256]{2,1,0:T(8,128)(2,1)} %param.19) | copy-start | bytes 1572868
  38.4 12.3 %all-to-all-start = ((f32[16,64,128]{2,1,0:T(8,128)}), f32[16,64,128]{2,1,0:T(8,128)S(1)}, u32[]{:S(2)}, u32[]{:S(2)}) async-start(f32[16,64,128]{2,1,0:T(8,128)} %bitcast.3), calls=%async_computation | async-start | bytes 1048576 | tf_op jit(solution)/shard_map/all_to_all | solution.py:118
  41.9 2.2 copy-start.12
  41.9 3.0 %copy-start.15 = (f32[4,256]{1,0:T(4,128)S(1)}, f32[4,256]{1,0:T(4,128)}, u32[]{:S(2)}) copy-start(f32[4,256]{1,0:T(4,128)} %param.20) | copy-start | bytes 12292
  44.9 1.1 copy-start.10
  44.9 1.6 copy-start.9
  44.9 3.2 %copy-start.13 = (bf16[4,256,128]{2,1,0:T(8,128)(2,1)S(1)}, bf16[4,256,128]{2,1,0:T(8,128)(2,1)}, u32[]{:S(2)}) copy-start(bf16[4,256,128]{2,1,0:T(8,128)(2,1)} %param.17) | copy-start | bytes 786436
  51.4 19.0 %all-to-all-start.1 = ((bf16[16,64,256]{2,1,0:T(8,128)(2,1)}), bf16[16,64,256]{2,1,0:T(8,128)(2,1)}, u32[]{:S(2)}, u32[]{:S(2)}) async-start(bf16[16,64,256]{2,1,0:T(8,128)(2,1)} %bitcast.16), calls=%async_computation.1 | async-start | bytes 1048576 | tf_op jit(solution)/shard_map/all_to_all | solution.py:124
  75.1 1.3 copy-start.1
  81.7 1.8 copy-start.6
  82.7 2.1 copy-start.2
  83.9 0.8 copy-start.7
  84.7 1.3 copy-start.1
  91.3 1.8 copy-start.6
  92.3 2.1 copy-start.2
  94.3 1.3 copy-start.1
  100.9 1.8 copy-start.6
  101.9 2.1 copy-start.2
  104.0 1.3 copy-start.1
  110.6 1.8 copy-start.6
  111.5 2.1 copy-start.2
  113.6 5.8 %copy-start.4 = (f32[4,4,64,128]{3,2,0,1:T(8,128)S(1)}, f32[4,4,64,128]{3,2,0,1:T(8,128)}, u32[]{:S(2)}) copy-start(f32[4,4,64,128]{3,2,0,1:T(8,128)} %copy.101) | copy-start | bytes 1572868
  119.3 5.1 %copy-start.3 = (f32[4,4,64,128]{3,2,0,1:T(8,128)S(1)}, f32[4,4,64,128]{3,2,0,1:T(8,128)}, u32[]{:S(2)}) copy-start(f32[4,4,64,128]{3,2,0,1:T(8,128)} %get-tuple-element.306) | copy-start | bytes 1572868
  120.8 9.5 %all-to-all-start.5 = ((bf16[4,256,128]{2,0,1:T(4,128)(2,1)}), bf16[4,256,128]{2,0,1:T(4,128)(2,1)S(1)}, u32[]{:S(2)}, u32[]{:S(2)}) async-start(bf16[4,256,128]{2,0,1:T(4,128)(2,1)} %copy.126), calls=%async_computation.5 | async-start | bytes 524288 | tf_op jit(solution)/shard_map/all_to_all | solution.py:139
  124.3 9.6 %copy-start.14 = (bf16[32,1024]{1,0:T(8,128)(2,1)S(1)}, bf16[32,1024]{1,0:T(8,128)(2,1)}, u32[]{:S(2)}) copy-start(bf16[32,1024]{1,0:T(8,128)(2,1)} %param.15) | copy-start | bytes 196612
  130.3 9.4 %all-to-all-start.2 = ((bf16[4,256,128]{2,0,1:T(4,128)(2,1)}), bf16[4,256,128]{2,0,1:T(4,128)(2,1)S(1)}, u32[]{:S(2)}, u32[]{:S(2)}) async-start(bf16[4,256,128]{2,0,1:T(4,128)(2,1)} %copy.111), calls=%async_computation.2 | async-start | bytes 524288 | tf_op jit(solution)/shard_map/all_to_all | solution.py:136
  133.7 10.3 %copy-start.8 = (bf16[4,4,64,256]{3,2,0,1:T(8,128)(2,1)S(1)}, bf16[4,4,64,256]{3,2,0,1:T(8,128)(2,1)}, u32[]{:S(2)}) copy-start(bf16[4,4,64,256]{3,2,0,1:T(8,128)(2,1)} %get-tuple-element.308) | copy-start | bytes 1572868
  139.7 9.4 %all-to-all-start.3 = ((bf16[4,256,128]{2,0,1:T(4,128)(2,1)}), bf16[4,256,128]{2,0,1:T(4,128)(2,1)S(1)}, u32[]{:S(2)}, u32[]{:S(2)}) async-start(bf16[4,256,128]{2,0,1:T(4,128)(2,1)} %copy.116), calls=%async_computation.3 | async-start | bytes 524288 | tf_op jit(solution)/shard_map/all_to_all | solution.py:137
  143.1 80.8 %all-reduce.7.cloned.1.call-start = ((), (), s32[]{:S(2)}) async-start(), calls=%async_computation.6 | async-start | bytes 819200 | tf_op jit(solution)/shard_map/psum | solution.py:162
  149.0 75.7 %all-to-all-start.4 = ((bf16[4,256,256]{2,0,1:T(4,128)(2,1)}), bf16[4,256,256]{2,0,1:T(4,128)(2,1)S(1)}, u32[]{:S(2)}, u32[]{:S(2)}) async-start(bf16[4,256,256]{2,0,1:T(4,128)(2,1)} %copy.121), calls=%async_computation.4 | async-start | bytes 1048576 | tf_op jit(solution)/shard_map/all_to_all | solution.py:138
  152.5 106.2 %all-reduce.9.cloned.1.call-start = ((), (), s32[]{:S(2)}) async-start(), calls=%async_computation.7 | async-start | bytes 819200 | tf_op jit(solution)/shard_map/psum | solution.py:161
  (4 other events, 3.2 us)
Sparse Core Ops, SparseCore 0:
  147.9 75.8 all-reduce.6
  226.3 32.4 all-reduce.8
